TPU v7x, 32 devices: a whole 2x2x4 slice. The times are simulated.
32 devices in a mesh: rep: 4 (over z), fs: 4 (over y, x), tp: 2 (over core).
Axes of the slice: x: 2, y: 2, z: 4, core: 2. Of those that a mesh axis runs over, the one named last changes fastest.
Arguments:
- tokens: bfloat16 [4096, 2048], P(('rep', 'fs', 'tp')), may hold values from -6 to 6
- cotangent: bfloat16 [4096, 2048], P(('rep', 'fs', 'tp')), may hold values from -6 to 6
- gate_weight: bfloat16 [2048, 3072], P(None, 'fs'), may hold values from -0.125 to 0.125
- up_weight: bfloat16 [2048, 3072], P(None, 'fs'), may hold values from -0.125 to 0.125
- down_weight_t: bfloat16 [2048, 3072], P(None, 'fs'), may hold values from -0.109375 to 0.109375
Outputs:
- input_grad: bfloat16 [4096, 2048], P(('rep', 'fs', 'tp'))
- gate_grad: float32 [2048, 3072], P(('rep', 'tp'), 'fs')
- up_grad: float32 [2048, 3072], P(('rep', 'tp'), 'fs')
- down_grad: float32 [2048, 3072], P(('rep', 'tp'), 'fs')
All inputs are finite; a program needn't handle non-finite values.
Results may differ from a plain program's by a relative error of at most 0.012.
Values may be sent and summed in bfloat16 or wider, within the bound.
A program may use at most 128 MiB of HBM per device.

v0:
```python
import jax
import jax.numpy as jnp
from jax import lax
from jax.sharding import PartitionSpec as P


def on_device(tokens, cotangent, gate_weight, up_weight, down_weight_t):
    tok_rows, cot_rows = lax.all_gather((tokens, cotangent), "fs", axis=0, tiled=True)
    gate_pre = jnp.dot(tok_rows, gate_weight, preferred_element_type=jnp.float32)
    up_pre = jnp.dot(tok_rows, up_weight, preferred_element_type=jnp.float32)
    sig_gate = jax.nn.sigmoid(gate_pre)
    act_gate = gate_pre * sig_gate
    hidden = (act_gate * up_pre).astype(jnp.bfloat16)
    hid_grad = jnp.dot(cot_rows, down_weight_t, preferred_element_type=jnp.float32)
    local_gate_back = (hid_grad * up_pre * sig_gate * (1.0 + gate_pre * (1.0 - sig_gate))).astype(
        jnp.bfloat16
    )
    local_up_back = (hid_grad * act_gate).astype(jnp.bfloat16)
    tok_all, cot_all, gate_back, up_back, hidden = (
        tok_rows,
        cot_rows,
        local_gate_back,
        local_up_back,
        hidden,
    )
    own_rows = tokens.shape[0]
    across = (((1,), (1,)), ((), ()))
    input_grad = lax.psum_scatter(
        (
            lax.dot_general(gate_back, gate_weight, across, preferred_element_type=jnp.float32)
            + lax.dot_general(up_back, up_weight, across, preferred_element_type=jnp.float32)
        ).astype(jnp.bfloat16),
        "fs",
        scatter_dimension=0,
        tiled=True,
    )
    replicas = lax.axis_size("rep")
    cores = lax.axis_size("tp")
    shards = lax.axis_size("fs")
    grad_scale = float(own_rows * replicas * shards * cores) ** (-0.5)
    features = tok_all.shape[1]
    row_span = features // (replicas * cores)
    tok_order = tok_all.reshape(-1, replicas, cores, row_span).swapaxes(1, 2).reshape(-1, features)
    cot_order = cot_all.reshape(-1, replicas, cores, row_span).swapaxes(1, 2).reshape(-1, features)
    down_rows = (((0,), (0,)), ((), ()))
    gate_local = (
        lax.dot_general(tok_order, gate_back, down_rows, preferred_element_type=jnp.float32)
        * grad_scale
    )
    up_local = (
        lax.dot_general(tok_order, up_back, down_rows, preferred_element_type=jnp.float32)
        * grad_scale
    )
    down_local = (
        lax.dot_general(cot_order, hidden, down_rows, preferred_element_type=jnp.float32)
        * grad_scale
    )
    section_one = (
        lax.psum_scatter(
            gate_local.astype(jnp.bfloat16), "tp", scatter_dimension=0, tiled=True
        ).astype(jnp.float32),
        lax.psum_scatter(
            up_local.astype(jnp.bfloat16), "tp", scatter_dimension=0, tiled=True
        ).astype(jnp.float32),
        lax.psum_scatter(
            down_local.astype(jnp.bfloat16), "tp", scatter_dimension=0, tiled=True
        ).astype(jnp.float32),
    )
    summed = (
        lax.psum_scatter(
            section_one[0].astype(jnp.bfloat16), "rep", scatter_dimension=0, tiled=True
        ).astype(jnp.float32),
        lax.psum_scatter(
            section_one[1].astype(jnp.bfloat16), "rep", scatter_dimension=0, tiled=True
        ).astype(jnp.float32),
        lax.psum_scatter(
            section_one[2].astype(jnp.bfloat16), "rep", scatter_dimension=0, tiled=True
        ).astype(jnp.float32),
    )
    return (input_grad, summed[0], summed[1], summed[2])


def solution(mesh):
    return jax.shard_map(
        on_device,
        mesh=mesh,
        in_specs=(
            P(("rep", "fs", "tp"), None),
            P(("rep", "fs", "tp"), None),
            P(None, "fs"),
            P(None, "fs"),
            P(None, "fs"),
        ),
        out_specs=(
            P(("rep", "fs", "tp"), None),
            P(("rep", "tp"), "fs"),
            P(("rep", "tp"), "fs"),
            P(("rep", "tp"), "fs"),
        ),
        check_vma=False,
    )
```

profile of v0, /device:TPU:0, one launch (start us, length us, event | category | flops | bytes accessed | tf_op | source)
XLA Modules:
  0.0 292.1 jit_solution(12534820842783169199)
XLA Ops:
  7.2 2.2 copy.15
  9.4 0.0 all-gather.5.cloned.1.call-start
  9.5 2.0 copy.16
  11.6 0.0 reduce-scatter.18.cloned.1.call-start
  11.6 36.6 %all-gather.3.cloned.1.call-done = bf16[512,2048]{0,1:T(8,128)(2,1)} async-done(((bf16[128,2048]{0,1:T(8,128)(2,1)}), bf16[512,2048]{0,1:T(8,128)(2,1)}) %all-gather.3.cloned.1.call-update) | async-done | bytes 2097168 | tf_op jit(solution)/shard_map/all_gather | solution.py:8
  48.2 3.1 %copy.18 = bf16[512,2,4,256]{0,3,2,1:T(8,128)(2,1)} copy(bf16[512,2,4,256]{0,3,1,2:T(8,128)(2,1)} %bitcast.29) | data formatting | bytes 4194304 | tf_op jit(solution)/shard_map/transpose | solution.py:44
  51.3 34.4 %all-gather.5.cloned.1.call-done = bf16[512,2048]{0,1:T(8,128)(2,1)} async-done(((bf16[128,2048]{0,1:T(8,128)(2,1)}), bf16[512,2048]{0,1:T(8,128)(2,1)}) %all-gather.5.cloned.1.call-update) | async-done | bytes 2097168 | tf_op jit(solution)/shard_map/all_gather | solution.py:8
  85.7 3.6 %fusion.7 = f32[512,768]{1,0:T(8,128)S(1)} fusion(bf16[512,2048]{0,1:T(8,128)(2,1)} %all-gather.5.cloned.1.call-done, bf16[2048,768]{1,0:T(8,128)(2,1)S(1)} %copy-done), kind=kOutput, calls=%fused_computation.14 | convolution fusion | flops 1610612736 | bytes 6815744 | tf_op jit(solution)/shard_map/dot_general | solution.py:9
  89.3 1.9 fusion.6
  91.2 1.2 copy-done.11
  92.4 3.6 %fusion.2 = bf16[2048,768]{0,1:T(8,128)(2,1)} fusion(bf16[512,2048]{0,1:T(8,128)(2,1)S(1)} %bitcast.33, f32[512,768]{1,0:T(8,128)S(1)} %fusion.6, f32[512,768]{1,0:T(8,128)S(1)} %fusion.7), kind=kOutput, calls=%fused_computation.6 | convolution fusion | flops 1616117760 | bytes 8388608 | tf_op jit(solution)/shard_map/dot_general | solution.py:55
  96.1 2.0 copy.17
  98.0 0.2 copy-done.1
  98.3 0.4 copy-done.10
  98.7 6.3 %multiply_convert_fusion.4 = (bf16[512,768]{1,0:T(8,128)(2,1)S(1)}, bf16[512,768]{1,0:T(8,128)(2,1)}) fusion(f32[512,768]{1,0:T(8,128)S(1)} %copy-done.10, f32[512,768]{1,0:T(8,128)} %copy-done.11, bf16[512,2048]{0,1:T(8,128)(2,1)S(1)} %copy-done.1, bf16[2048,768]{1,0:T(8,128)(2,1)} %param.9), kind=kOutput, calls=%fused_computation.8 | convolution fusion | flops 1615724544 | bytes 9961472 | tf_op jit(solution)/shard_map/dot_general | solution.py:14
  105.0 0.9 copy-done.7
  105.9 3.6 %fusion.1 = bf16[2048,768]{0,1:T(8,128)(2,1)} fusion(bf16[512,768]{1,0:T(8,128)(2,1)S(1)} %get-tuple-element.16, bf16[512,2048]{0,1:T(8,128)(2,1)S(1)} %bitcast.31), kind=kOutput, calls=%fused_computation.5 | convolution fusion | flops 1613758464 | bytes 6029312 | tf_op jit(solution)/shard_map/dot_general | solution.py:51
  109.5 0.0 reduce-scatter.10.cloned.1.call-start
  109.5 5.4 %fusion = bf16[2048,768]{0,1:T(8,128)(2,1)} fusion(bf16[512,768]{1,0:T(8,128)(2,1)} %get-tuple-element.17, bf16[512,2048]{0,1:T(8,128)(2,1)} %bitcast.32), kind=kOutput, calls=%fused_computation.4 | convolution fusion | flops 1613758464 | bytes 6029312 | tf_op jit(solution)/shard_map/dot_general | solution.py:47
  115.0 0.5 reduce-scatter.20.cloned.1.call-update
  115.5 0.2 reduce-scatter.16.cloned.1.call-start
  115.7 5.7 %reduce-scatter.14.cloned.1.call-done = bf16[1024,768]{0,1:T(8,128)(2,1)} async-done(((bf16[2048,768]{0,1:T(8,128)(2,1)}), bf16[1024,768]{0,1:T(8,128)(2,1)}) %reduce-scatter.14.cloned.1.call-update) | async-done | bytes 1572880 | tf_op jit(solution)/shard_map/reduce_scatter | solution.py:62
  121.5 14.3 %reduce-scatter.10.cloned.1.call-done = bf16[1024,768]{0,1:T(8,128)(2,1)} async-done(((bf16[2048,768]{0,1:T(8,128)(2,1)}), bf16[1024,768]{0,1:T(8,128)(2,1)}) %reduce-scatter.10.cloned.1.call-update) | async-done | bytes 1572880 | tf_op jit(solution)/shard_map/reduce_scatter | solution.py:59
  135.9 3.1 %fusion.8 = f32[512,2048]{1,0:T(8,128)S(1)} fusion(bf16[512,768]{1,0:T(8,128)(2,1)} %get-tuple-element.17, bf16[2048,768]{1,0:T(8,128)(2,1)S(1)} %copy-done), kind=kOutput, calls=%fused_computation.15 | convolution fusion | flops 1610612736 | bytes 8126464 | tf_op jit(solution)/shard_map/dot_general | solution.py:30
  139.0 3.2 %add_convert_fusion = bf16[512,2048]{1,0:T(8,128)(2,1)} fusion(f32[512,2048]{1,0:T(8,128)S(1)} %fusion.8, bf16[512,768]{1,0:T(8,128)(2,1)S(1)} %copy-done.8, bf16[2048,768]{1,0:T(8,128)(2,1)S(1)} %copy-done.6), kind=kOutput, calls=%fused_computation.3 | convolution fusion | flops 1612709888 | bytes 10223616 | tf_op jit(solution)/shard_map/dot_general | solution.py:31
  142.2 32.5 %reduce-scatter.20.cloned.1.call-done = bf16[256,768]{0,1:T(8,128)(2,1)} async-done(((bf16[1024,768]{0,1:T(8,128)(2,1)}), bf16[256,768]{0,1:T(8,128)(2,1)}) %reduce-scatter.20.cloned.1.call-update) | async-done | bytes 393232 | tf_op jit(solution)/shard_map/reduce_scatter | solution.py:76
  174.8 2.0 copy.21
  176.8 34.6 %reduce-scatter.16.cloned.1.call-done = bf16[256,768]{0,1:T(8,128)(2,1)} async-done(((bf16[1024,768]{0,1:T(8,128)(2,1)}), bf16[256,768]{0,1:T(8,128)(2,1)}) %reduce-scatter.16.cloned.1.call-update) | async-done | bytes 393232 | tf_op jit(solution)/shard_map/reduce_scatter | solution.py:73
  211.4 2.0 copy.20
  213.4 34.6 %reduce-scatter.12.cloned.1.call-done = bf16[256,768]{0,1:T(8,128)(2,1)} async-done(((bf16[1024,768]{0,1:T(8,128)(2,1)}), bf16[256,768]{0,1:T(8,128)(2,1)}) %reduce-scatter.12.cloned.1.call-update) | async-done | bytes 393232 | tf_op jit(solution)/shard_map/reduce_scatter | solution.py:70
  248.0 2.0 copy.19
  250.0 35.5 %reduce-scatter.8.cloned.1.call-done = bf16[128,2048]{1,0:T(8,128)(2,1)} async-done(((bf16[512,2048]{1,0:T(8,128)(2,1)}), bf16[128,2048]{1,0:T(8,128)(2,1)}) %reduce-scatter.8.cloned.1.call-update) | async-done | bytes 524304 | tf_op jit(solution)/shard_map/reduce_scatter | solution.py:28
  (34 shorter events, 0.4 us)
Async XLA Ops:
  7.2 78.5 %copy-start = (bf16[2048,768]{1,0:T(8,128)(2,1)S(1)}, bf16[2048,768]{1,0:T(8,128)(2,1)}, u32[]{:S(2)}) copy-start(bf16[2048,768]{1,0:T(8,128)(2,1)} %param.7) | copy-start | bytes 9437188
  7.2 41.0 %all-gather.3.cloned.1.call-start = ((), (), s32[]{:S(2)}) async-start(), calls=%async_computation.7 | async-start | bytes 2621440 | tf_op jit(solution)/shard_map/all_gather | solution.py:8
  9.4 76.2 %all-gather.5.cloned.1.call-start = ((), (), s32[]{:S(2)}) async-start(), calls=%async_computation.8 | async-start | bytes 2621440 | tf_op jit(solution)/shard_map/all_gather | solution.py:8
  11.6 103.4 %reduce-scatter.18.cloned.1.call-start = ((), (), s32[]{:S(2)}) async-start(), calls=%async_computation.14 | async-start | bytes 4718592 | tf_op jit(solution)/shard_map/reduce_scatter | solution.py:65
  85.7 3.6 %copy-start.2 = (bf16[512,2048]{0,1:T(8,128)(2,1)S(1)}, bf16[512,2048]{0,1:T(8,128)(2,1)}, u32[]{:S(2)}) copy-start(bf16[512,2048]{0,1:T(8,128)(2,1)} %all-gather.5.cloned.1.call-done) | copy-start | bytes 6291460
  85.7 3.6 %copy-start.5 = (bf16[2048,768]{1,0:T(8,128)(2,1)S(1)}, bf16[2048,768]{1,0:T(8,128)(2,1)}, u32[]{:S(2)}) copy-start(bf16[2048,768]{1,0:T(8,128)(2,1)} %param.8) | copy-start | bytes 9437188
  89.3 1.9 copy-start.9
  89.3 3.1 %copy-start.4 = (bf16[512,2,4,256]{0,3,2,1:T(8,128)(2,1)S(1)}, bf16[512,2,4,256]{0,3,2,1:T(8,128)(2,1)}, u32[]{:S(2)}) copy-start(bf16[512,2,4,256]{0,3,2,1:T(8,128)(2,1)} %copy.18) | copy-start | bytes 6291460
  91.2 1.2 copy-start.11
  96.0 25.5 %reduce-scatter.14.cloned.1.call-start = ((), (), s32[]{:S(2)}) async-start(), calls=%async_computation.12 | async-start | bytes 4718592 | tf_op jit(solution)/shard_map/reduce_scatter | solution.py:62
  96.0 2.2 copy-start.1
  96.0 2.7 copy-start.10
  98.7 6.3 %copy-start.3 = (bf16[512,2,4,256]{0,3,2,1:T(8,128)(2,1)}, bf16[512,2,4,256]{0,3,2,1:T(8,128)(2,1)S(1)}, u32[]{:S(2)}) copy-start(bf16[512,2,4,256]{0,3,2,1:T(8,128)(2,1)S(1)} %copy.17) | copy-start | bytes 6291460
  105.0 0.9 copy-start.7
  109.5 26.3 %reduce-scatter.10.cloned.1.call-start = ((), (), s32[]{:S(2)}) async-start(), calls=%async_computation.10 | async-start | bytes 4718592 | tf_op jit(solution)/shard_map/reduce_scatter | solution.py:59
  114.9 59.8 %reduce-scatter.20.cloned.1.call-start = ((), (), s32[]{:S(2)}) async-start(), calls=%async_computation.15 | async-start | bytes 1966080 | tf_op jit(solution)/shard_map/reduce_scatter | solution.py:76
  115.5 95.9 %reduce-scatter.16.cloned.1.call-start = ((), (), s32[]{:S(2)}) async-start(), calls=%async_computation.13 | async-start | bytes 1966080 | tf_op jit(solution)/shard_map/reduce_scatter | solution.py:73
  121.5 126.5 %reduce-scatter.12.cloned.1.call-start = ((), (), s32[]{:S(2)}) async-start(), calls=%async_computation.11 | async-start | bytes 1966080 | tf_op jit(solution)/shard_map/reduce_scatter | solution.py:70
  135.8 149.7 %reduce-scatter.8.cloned.1.call-start = ((), (), s32[]{:S(2)}) async-start(), calls=%async_computation.9 | async-start | bytes 2621440 | tf_op jit(solution)/shard_map/reduce_scatter | solution.py:28
  135.9 3.1 %copy-start.6 = (bf16[2048,768]{1,0:T(8,128)(2,1)S(1)}, bf16[2048,768]{1,0:T(8,128)(2,1)}, u32[]{:S(2)}) copy-start(bf16[2048,768]{1,0:T(8,128)(2,1)} %param.8) | copy-start | bytes 9437188
  135.9 3.1 %copy-start.8 = (bf16[512,768]{1,0:T(8,128)(2,1)S(1)}, bf16[512,768]{1,0:T(8,128)(2,1)}, u32[]{:S(2)}) copy-start(bf16[512,768]{1,0:T(8,128)(2,1)} %copy-done.7) | copy-start | bytes 2359300
Sparse Core Ops, SparseCore 0:
  10.4 37.7 all-gather.2
  50.6 35.0 all-gather.4
  96.1 10.9 reduce-scatter.17
  109.6 11.8 reduce-scatter.13
  123.5 12.2 reduce-scatter.9
  138.0 36.7 reduce-scatter.19
  177.1 34.2 reduce-scatter.15
  213.7 34.2 reduce-scatter.11
  251.5 33.9 reduce-scatter.7
where the time goes:
time: 292 us
  waiting for transfers between devices  229 us (78%)
  matrix products  30.5 us (10%)
  local copies, waits for them, and re-layouts  18.2 us (6%)
  between operations  14 us (5%)
    all_gather x2, waiting for transfers between devices, on_device(): lax.all_gather((tokens, cotangent), 'fs', axis=0, tiled=True)  71 us
    reduce_scatter x1, waiting for transfers between devices, on_device(): lax.psum_scatter((lax.dot_general(gate_back, gate_weight, across, preferr...  35.5 us
    reduce_scatter x1, waiting for transfers between devices, on_device(): lax.psum_scatter(section_one[1].astype(jnp.bfloat16), 'rep', scatter_dime...  34.6 us
    reduce_scatter x1, waiting for transfers between devices, on_device(): lax.psum_scatter(section_one[0].astype(jnp.bfloat16), 'rep', scatter_dime...  34.6 us
    reduce_scatter x1, waiting for transfers between devices, on_device(): lax.psum_scatter(section_one[2].astype(jnp.bfloat16), 'rep', scatter_dime...  32.5 us
    reduce_scatter x1, waiting for transfers between devices, on_device(): lax.psum_scatter(gate_local.astype(jnp.bfloat16), 'tp', scatter_dimension...  14.3 us
    unnamed x29, local copies, waits for them, and re-layouts  13.2 us
    dot_general x1, matrix products, on_device(): jnp.dot(cot_rows, down_weight_t, preferred_element_type=jnp.float32)  6.3 us
  transfers between devices with their start and end apart: 9, of which 8 were waited for; matrix products, arithmetic and copies ran while one was open for 12% of the time, Pallas kernels for 0%

commit v1 on v0

v1 whole, which is shorter than its diff:
```python
import functools

import jax
import jax.numpy as jnp
from jax import lax
from jax.experimental import pallas as pl
from jax.experimental.pallas import tpu as pltpu
from jax.sharding import PartitionSpec as P

MESH = pl.DeviceIdType.MESH
F32 = jnp.float32
BF16 = jnp.bfloat16


def tile_of(size, want=256):
    return want if size % want == 0 else size


def kernel(
    n_rep, n_tp, grad_scale,
    tok_hbm, cot_hbm, gw_hbm, uw_hbm, dw_hbm,
    igrad, ggrad, ugrad, dgrad,
    tok, cot, gw, uw, dw, tok_t, cot_t, gb, ub, hd, part, part_in, out_buf, in_buf,
    load_sem, g_send, g_recv, c_send, c_recv, p_send, p_recv, r_send, r_recv,
):
    slots, rows, features = tok.shape
    hidden = gb.shape[1]
    span = features // (n_rep * n_tp)
    half = hidden // 2
    me_r = lax.axis_index("rep")
    f = lax.axis_index("fs")
    t = lax.axis_index("tp")
    side = f + 1 - 2 * (f % 2)
    up = (f + 2) % 4
    diag = (side + 2) % 4
    peers = (None, side, up, diag)
    right = (me_r + 1) % n_rep
    left = (me_r + n_rep - 1) % n_rep
    twin = 1 - t

    def local(src, dst, i):
        return pltpu.make_async_copy(src, dst, load_sem.at[i])

    loads = [
        local(tok_hbm, tok.at[0], 0),
        local(cot_hbm, cot.at[0], 1),
        local(gw_hbm, gw, 2),
        local(uw_hbm, uw, 3),
        local(dw_hbm, dw, 4),
    ]
    for c in loads:
        c.start()

    barrier = pltpu.get_barrier_semaphore()
    targets = [{"fs": side}, {"fs": up}, {"fs": diag}, {"rep": right}, {"rep": left}, {"tp": twin}]
    for d in targets:
        pl.semaphore_signal(barrier, inc=1, device_id=d, device_id_type=MESH)
    pl.semaphore_wait(barrier, len(targets))

    def remote(src, dst, ss, rs, dev):
        return pltpu.make_async_remote_copy(
            src_ref=src, dst_ref=dst, send_sem=ss, recv_sem=rs, device_id=dev, device_id_type=MESH
        )

    def gather(i, src, dst, dev):
        return remote(src, dst, g_send.at[i], g_recv.at[i], {"fs": dev})

    cot_x = gather(0, cot_hbm, cot.at[1], side)
    tok_y = gather(1, tok_hbm, tok.at[2], up)
    tok_x = gather(2, tok_hbm, tok.at[1], side)
    cot_y = gather(3, cot_hbm, cot.at[2], up)
    tok_d = gather(4, tok.at[2], tok.at[3], side)
    cot_d = gather(5, cot.at[1], cot.at[3], up)
    for c in (cot_x, tok_y, tok_x, cot_y):
        c.start()

    def cross(k, i, src, dst):
        return remote(src, dst, c_send.at[k, i], c_recv.at[k, i], {"tp": twin})

    def crossings(k):
        here, there = slice(k * rows, (k + 1) * rows), slice((slots + k) * rows, (slots + k + 1) * rows)
        return [
            cross(k, 0, tok_t.at[:, here], tok_t.at[:, there]),
            cross(k, 1, cot_t.at[:, here], cot_t.at[:, there]),
            cross(k, 2, gb.at[here], gb.at[there]),
            cross(k, 3, ub.at[here], ub.at[there]),
            cross(k, 4, hd.at[here], hd.at[there]),
        ]

    def turn(k, src, dst):
        width = tile_of(features)

        @pl.loop(0, features // width)
        def _(j):
            piece = pl.ds(pl.multiple_of(j * width, width), width)
            dst[piece, k * rows:(k + 1) * rows] = src[k, :, piece].T

    def forward(k):
        width = tile_of(hidden)
        here = slice(k * rows, (k + 1) * rows)

        @pl.loop(0, hidden // width)
        def _(j):
            cols = pl.ds(pl.multiple_of(j * width, width), width)
            g = jnp.dot(tok[k], gw[:, cols], preferred_element_type=F32)
            u = jnp.dot(tok[k], uw[:, cols], preferred_element_type=F32)
            h = jnp.dot(cot[k], dw[:, cols], preferred_element_type=F32)
            sig = jax.nn.sigmoid(g)
            act = g * sig
            hd[here, cols] = (act * u).astype(BF16)
            gb[here, cols] = (h * u * sig * (1.0 + g * (1.0 - sig))).astype(BF16)
            ub[here, cols] = (h * act).astype(BF16)

    def handle(k):
        sends = crossings(k)
        turn(k, tok, tok_t)
        sends[0].start()
        turn(k, cot, cot_t)
        sends[1].start()
        forward(k)
        for c in sends[2:]:
            c.start()

    for c in loads:
        c.wait()
    handle(0)
    cot_x.wait_recv()
    cot_d.start()
    tok_y.wait_recv()
    tok_d.start()
    tok_x.wait_recv()
    handle(1)
    cot_y.wait_recv()
    handle(2)
    tok_d.wait_recv()
    cot_d.wait_recv()
    handle(3)
    for k in range(slots):
        for c in crossings(k):
            c.wait_recv()

    pairs = ((tok_t, gb), (tok_t, ub), (cot_t, hd))
    outs = (ggrad, ugrad, dgrad)

    def dest(way, s):
        if way == 0:
            return (me_r + 2 * n_rep - 1 - s) % n_rep
        return (me_r + 1 + s) % n_rep

    def piece(way, s, a):
        lhs, rhs = pairs[a]
        band = pl.ds(pl.multiple_of((dest(way, s) * n_tp + t) * span, span), span)
        return jnp.dot(lhs[band, :], rhs[:, way * half:(way + 1) * half], preferred_element_type=F32)

    def hop(way, s, a):
        return remote(
            out_buf.at[way, s, a], in_buf.at[way, s, a],
            r_send.at[way, s, a], r_recv.at[way, s, a],
            {"rep": right if way == 0 else left},
        )

    for a in range(3):
        for way in range(2):
            out_buf[way, 0, a] = piece(way, 0, a).astype(BF16)
            hop(way, 0, a).start()

    width = tile_of(features)
    across = (((1,), (1,)), ((), ()))

    @pl.loop(0, features // width)
    def _(j):
        band = pl.ds(pl.multiple_of(j * width, width), width)
        total = lax.dot_general(gb[0:slots * rows], gw[band, :], across, preferred_element_type=F32)
        total = total + lax.dot_general(ub[0:slots * rows], uw[band, :], across, preferred_element_type=F32)
        part[:, :, band] = total.astype(BF16).reshape(slots, rows, width)

    def give(k):
        return remote(part.at[k], part_in.at[k - 1], p_send.at[k - 1], p_recv.at[k - 1], {"fs": peers[k]})

    for k in (3, 1, 2):
        give(k).start()

    @pl.loop(1, n_rep - 1)
    def _(s):
        for a in range(3):
            for way in range(2):
                own = piece(way, s, a)
                hop(way, s - 1, a).wait_recv()
                out_buf[way, s, a] = (own + in_buf[way, s - 1, a].astype(F32)).astype(BF16)
                hop(way, s, a).start()

    for k in (1, 2, 3):
        give(k).wait_recv()
    igrad[...] = (
        part[0].astype(F32) + part_in[0].astype(F32) + part_in[1].astype(F32) + part_in[2].astype(F32)
    ).astype(BF16)

    for a in range(3):
        for way in range(2):
            own = piece(way, n_rep - 1, a)
            hop(way, n_rep - 2, a).wait_recv()
            outs[a][:, way * half:(way + 1) * half] = (
                own + in_buf[way, n_rep - 2, a].astype(F32)
            ) * grad_scale

    for c in (cot_x, tok_y, tok_x, cot_y, tok_d, cot_d):
        c.wait_send()
    for k in range(slots):
        for c in crossings(k):
            c.wait_send()
    for k in (1, 2, 3):
        give(k).wait_send()

    @pl.loop(0, n_rep - 1)
    def _(s):
        for a in range(3):
            for way in range(2):
                hop(way, s, a).wait_send()


def solution(mesh):
    n_rep, n_fs, n_tp = (mesh.shape[a] for a in ("rep", "fs", "tp"))
    assert n_fs == 4 and n_tp == 2 and n_rep > 2

    def on_device(tokens, cotangent, gate_weight, up_weight, down_weight_t):
        rows, features = tokens.shape
        hidden = gate_weight.shape[1]
        span = features // (n_rep * n_tp)
        both = n_tp * n_fs * rows
        hops = (2, n_rep - 1, 3)
        anywhere = pl.BlockSpec(memory_space=pl.ANY)
        vmem = pl.BlockSpec(memory_space=pltpu.VMEM)
        dma = pltpu.SemaphoreType.DMA
        grad = jax.ShapeDtypeStruct((span, hidden), F32)
        scale = float(rows * n_rep * n_fs * n_tp) ** (-0.5)
        return pl.pallas_call(
            functools.partial(kernel, n_rep, n_tp, scale),
            out_shape=(jax.ShapeDtypeStruct((rows, features), BF16), grad, grad, grad),
            in_specs=[anywhere] * 5,
            out_specs=(vmem,) * 4,
            scratch_shapes=[
                pltpu.VMEM((n_fs, rows, features), BF16),
                pltpu.VMEM((n_fs, rows, features), BF16),
                pltpu.VMEM((features, hidden), BF16),
                pltpu.VMEM((features, hidden), BF16),
                pltpu.VMEM((features, hidden), BF16),
                pltpu.VMEM((features, both), BF16),
                pltpu.VMEM((features, both), BF16),
                pltpu.VMEM((both, hidden), BF16),
                pltpu.VMEM((both, hidden), BF16),
                pltpu.VMEM((both, hidden), BF16),
                pltpu.VMEM((n_fs, rows, features), BF16),
                pltpu.VMEM((n_fs - 1, rows, features), BF16),
                pltpu.VMEM(hops + (span, hidden // 2), BF16),
                pltpu.VMEM(hops + (span, hidden // 2), BF16),
                dma((5,)),
                dma((6,)),
                dma((6,)),
                dma((n_fs, 5)),
                dma((n_fs, 5)),
                dma((n_fs - 1,)),
                dma((n_fs - 1,)),
                dma(hops),
                dma(hops),
            ],
            compiler_params=pltpu.CompilerParams(
                collective_id=0, has_side_effects=True, vmem_limit_bytes=60 * 1024 * 1024
            ),
        )(tokens, cotangent, gate_weight, up_weight, down_weight_t)

    return jax.shard_map(
        on_device,
        mesh=mesh,
        in_specs=(
            P(("rep", "fs", "tp"), None),
            P(("rep", "fs", "tp"), None),
            P(None, "fs"),
            P(None, "fs"),
            P(None, "fs"),
        ),
        out_specs=(
            P(("rep", "fs", "tp"), None),
            P(("rep", "tp"), "fs"),
            P(("rep", "tp"), "fs"),
            P(("rep", "tp"), "fs"),
        ),
        check_vma=False,
    )
```

time: 292 us -> 131 us (0.45)
  waiting for transfers between devices: 229 us -> 0 us
  Pallas kernels: 0 us -> 124 us
  matrix products: 30.5 us -> 0 us
  between operations: 14 us -> 0.66 us
  local copies, waits for them, and re-layouts: 18.2 us -> 5.83 us
    reduce_scatter x7 -> x0, waiting for transfers between devices: 157 us -> none  [the longest x1 35.5 us: on_device(): lax.psum_scatter((lax.dot_general(gate_back, gate_weight, across, preferr...]
    pallas_call x0 -> x1, Pallas kernels: none -> 124 us  [on_device(): pl.pallas_call(functools.partial(kernel, n_rep, n_tp, scale), out_shape=(...]
    all_gather x2 -> x0, waiting for transfers between devices: 71 us -> none  [on_device(): lax.all_gather((tokens, cotangent), 'fs', axis=0, tiled=True)]
    dot_general x8 -> x0, matrix products: 30.5 us -> none  [the longest x1 6.3 us: on_device(): jnp.dot(cot_rows, down_weight_t, preferred_element_type=jnp.float32)]
    unnamed x29 -> x8, local copies, waits for them, and re-layouts: 13.2 us -> 5.83 us
    transpose x2 -> x0, local copies, waits for them, and re-layouts: 5.03 us -> none  [the longest x1 3.07 us: on_device(): cot_all.reshape(-1, replicas, cores, row_span).swapaxes(1, 2)]
  transfers between devices with their start and end apart: 9 -> 0, of which waited for: 8 -> 0; matrix products, arithmetic and copies ran while one was open for 12% -> 0% of each run, Pallas kernels for 0% -> 0%
where the time goes in v1:
time: 131 us
  Pallas kernels  124 us (95%)
  local copies, waits for them, and re-layouts  5.83 us (4%)
    pallas_call x1, Pallas kernels, on_device(): pl.pallas_call(functools.partial(kernel, n_rep, n_tp, scale), out_shape=(...  124 us
    unnamed x8, local copies, waits for them, and re-layouts  5.83 us

profile of v1, /device:TPU:0, one launch (start us, length us, event | category | flops | bytes accessed | tf_op | source)
XLA Modules:
  0.0 131.0 jit_solution(12718275513637812795)
XLA Ops:
  0.6 124.5 %shard_map.84 = (bf16[128,2048]{1,0:T(8,128)(2,1)}, f32[256,768]{1,0:T(8,128)}, f32[256,768]{1,0:T(8,128)}, f32[256,768]{1,0:T(8,128)}) custom-call(bf16[128,2048]{1,0:T(8,128)(2,1)} %tok_hbm.1, bf16[128,2048]{1,0:T(8,128)(2,1)} %cot_hbm.1, bf16[2048,768]{1,0:T(8,128)(2,1)} %gw_hbm.1, bf16[2048,768]{1,0:T(8,128)(2,1)} %uw_hbm.1, bf16[2048,768]{1,0:T(8,128)(2,1)} %dw_hbm.1), custom_call_target="tpu_custom_call" | custom-call | tf_op jit(solution)/shard_map/pallas_call | solution.py:236
  125.1 0.0 copy-start.1
  125.1 0.0 copy-start
  125.2 2.0 %copy.13 = bf16[128,2048]{1,0:T(8,128)(2,1)} copy(bf16[128,2048]{1,0:T(8,128)(2,1)} %get-tuple-element.8) | data formatting | bytes 1048576
  127.1 2.1 %copy.14 = f32[256,768]{1,0:T(8,128)} copy(f32[256,768]{1,0:T(8,128)} %get-tuple-element.9) | data formatting | bytes 1572864
  129.2 0.0 copy-done.1
  129.2 0.9 copy.15
  130.1 0.0 copy-done
  130.1 0.9 copy.16
Async XLA Ops:
  125.1 4.1 %copy-start.1 = (f32[256,768]{1,0:T(8,128)S(1)}, f32[256,768]{1,0:T(8,128)}, u32[]{:S(2)}) copy-start(f32[256,768]{1,0:T(8,128)} %get-tuple-element.10) | copy-start | bytes 2359300
  125.1 5.0 %copy-start = (f32[256,768]{1,0:T(8,128)S(1)}, f32[256,768]{1,0:T(8,128)}, u32[]{:S(2)}) copy-start(f32[256,768]{1,0:T(8,128)} %get-tuple-element.11) | copy-start | bytes 2359300
